TPU v7x, 32 devices: a whole 2x2x4 slice. The times are simulated.
32 devices in a mesh: sp: 8 (over z, y), tp: 4 (over x, core).
Axes of the slice: x: 2, y: 2, z: 4, core: 2. Of those that a mesh axis runs over, the one named last changes fastest.
Arguments:
- arriving_hidden_sum: bfloat16 [8192, 2048], P('sp'), may hold values from -40 to 40
- content_entries_clustered: bfloat16 [8192, 4096], P('sp', 'tp'), may hold values from -6 to 6
- leaving_switch_entries: bfloat16 [8192, 4096], P('sp', 'tp'), may hold values from -6 to 6
- linked_source_target_pairs: bfloat16 [8192, 8, 2, 128], P('sp', 'tp'), may hold values from -1.78125 to 1.78125
- raw_interval_length: bfloat16 [8192, 64], P('sp', 'tp'), may hold values from -5 to 5
- spike_extra_lognoise: float32 [8192, 64], P('sp', 'tp'), may hold values from -0.6 to 0
- content_filter_kernel: bfloat16 [4, 4096], P(None, 'tp'), may hold values from -3 to 3
- coupling_filter_kernel: bfloat16 [4, 8, 2, 128], P(None, 'tp'), may hold values from -3 to 3
- interval_shift_vector: float32 [64], P('tp'), may hold values from -0.5 to 0.5
- fading_speed_exponent: float32 [64], P('tp'), may hold values from -16 to -2.9
- skip_channel_factor: float32 [64], P('tp'), may hold values from 1 to 10
- cluster_rescale_vector: float32 [4096], P('tp'), may hold values from 0.1 to 1.9
- blender_final_tensor: bfloat16 [4096, 2048], P('tp'), may hold values from -0.09375 to 0.09375
- prelayer_rescale_vector: float32 [2048], replicated, may hold values from 0.1 to 1.9
- switching_linear_tensor: bfloat16 [2048, 5632], P('sp', 'tp'), may hold values from -0.125 to 0.125
- widening_linear_tensor: bfloat16 [2048, 5632], P('sp', 'tp'), may hold values from -0.125 to 0.125
- contracting_linear_tensor: bfloat16 [5632, 2048], P('tp', 'sp'), may hold values from -0.078125 to 0.078125
Outputs:
- residual_out: bfloat16 [8192, 2048], P('sp', 'tp')
All inputs are finite; a program needn't handle non-finite values.
Results may differ from a plain program's by a relative error of at most 0.012.
Values may be sent and summed in bfloat16 or wider, within the bound.
A program may use at most 128 MiB of HBM per device.

v0:
```python
import jax
import jax.numpy as jnp
from jax import lax
from jax.experimental import pallas as pl
from jax.experimental.pallas import tpu as pltpu
from jax.sharding import PartitionSpec as P

BLOCK = 128
CORES = 2
EPS = 1e-06
HALO = 16
HIGHEST = lax.Precision.HIGHEST
MESH = pl.DeviceIdType.MESH
VMEM_BYTES = 66_000_000


def ring_shape(count):
    inner = 1
    while inner * inner * 4 <= count:
        inner *= 2
    outer = count // inner
    if inner == 1 or outer % 2:
        return count, 1
    return outer, inner


def ring_at(spot, count):
    outer, inner = ring_shape(count)
    if inner == 1:
        return spot
    if inner == 2:
        late = spot // outer
        return (1 - late) * spot * 2 + late * (2 * (count - 1 - spot) + 1)
    late = jnp.minimum(spot // outer, 1)
    rest = (spot - outer) * late
    lap, step = rest // (inner - 1), rest % (inner - 1)
    odd = lap % 2
    column = (1 + step) * (1 - odd) + (inner - 1 - step) * odd
    return (1 - late) * spot * inner + late * ((outer - 1 - lap) * inner + column)


def ring_spot(index, count):
    outer, inner = ring_shape(count)
    if inner == 1:
        return index
    plane, column = index // inner, index % inner
    late = jnp.minimum(column, 1)
    lap = outer - 1 - plane
    odd = lap % 2
    step = (column - 1) * (1 - odd) + (inner - 1 - column) * odd
    return (1 - late) * plane + late * (outer + lap * (inner - 1) + step)


class Ring:
    def __init__(self, pieces, send_sem, recv_sem):
        count = lax.axis_size("sp")
        me = lax.axis_index("sp")
        spot = ring_spot(me, count)
        self.count, self.hops, self.spot = count, count // 2, spot
        self.pieces, self.send_sem, self.recv_sem = pieces, send_sem, recv_sem
        self.next = (
            ring_at(lax.rem(spot + 1, count), count),
            ring_at(lax.rem(spot + count - 1, count), count),
        )

    def owner(self, way, hop):
        shift = self.count - hop if way == 0 else hop
        return ring_at(lax.rem(self.spot + shift, self.count), self.count)

    def active(self, piece, way, hop):
        return 2 * hop < self.count or piece % 2 == way

    def copy(self, piece, way, hop):
        src, dst = self.pieces[piece](hop == 1, self.owner(way, hop - 1))
        return pltpu.make_async_remote_copy(
            src_ref=src,
            dst_ref=dst,
            send_sem=self.send_sem.at[piece, way, hop - 1],
            recv_sem=self.recv_sem.at[piece, way, hop - 1],
            device_id={"sp": self.next[way]},
            device_id_type=MESH,
        )

    def start(self, piece, hop):
        for way in range(2):
            if self.active(piece, way, hop):
                self.copy(piece, way, hop).start()

    def arrive(self, piece, hop):
        for way in range(2):
            if self.active(piece, way, hop):
                self.copy(piece, way, hop).wait_recv()

    def forward(self, piece, hop):
        self.arrive(piece, hop - 1)
        self.start(piece, hop)

    def drain(self):
        for hop in range(1, self.hops + 1):
            for piece in range(len(self.pieces)):
                for way in range(2):
                    if self.active(piece, way, hop):
                        self.copy(piece, way, hop).wait_send()


def greet(others):
    barrier = pltpu.get_barrier_semaphore()
    for other in others:
        pl.semaphore_signal(barrier, inc=1, device_id=other, device_id_type=MESH)
    pl.semaphore_wait(barrier, len(others))


def peers():
    tp = lax.axis_index("tp")
    chips = lax.axis_size("tp") // CORES
    chip, core = tp // CORES, tp % CORES
    partner = {"tp": chip * CORES + 1 - core}
    across = [{"tp": lax.rem(chip + s, chips) * CORES + core} for s in range(1, chips)]
    return chip, core, partner, across


def silu(x):
    return x / (1.0 + jnp.exp(-x))


def dot(a, b, dims=((1,), (0,)), precision=None):
    return lax.dot_general(
        a, b, (dims, ((), ())), precision=precision, preferred_element_type=jnp.float32
    )


def mixer_kernel(
    arriving, content, leaving, pairs, gate_own, up_own, blend_hbm,
    raw, spike, value_taps, map_taps, shift, fading, skip, rescale,
    mid_out, gate_all, up_all,
    padded, map_padded, leave, blend, arrived, read_maps, mixer, mixed, state, reach, prior,
    messages, partial, from_partner, from_across, mid,
    local_sem, halo_sem, ring_send, ring_recv, state_send, state_recv,
    core_sem, across_sem, mid_sem, out_sem,
):
    length, channels = content.shape
    heads = raw.shape[1]
    size = channels // heads
    groups = read_maps.shape[1] // BLOCK
    wide = channels // groups
    per_group = heads // groups
    taps = value_taps.shape[0]
    blocks = length // BLOCK
    half = length // CORES
    count = lax.axis_size("sp")
    me = lax.axis_index("sp")
    chip, core, partner, across = peers()

    loads = [
        pltpu.make_async_copy(content, padded.at[HALO:], local_sem.at[0]),
        pltpu.make_async_copy(pairs, map_padded.at[HALO:], local_sem.at[1]),
        pltpu.make_async_copy(leaving, leave, local_sem.at[2]),
        pltpu.make_async_copy(blend_hbm, blend, local_sem.at[3]),
        pltpu.make_async_copy(
            arriving.at[pl.ds(pl.multiple_of(core * half, half), half)], arrived, local_sem.at[4]
        ),
    ]
    for load in loads:
        load.start()

    def weight(own, slots):
        return lambda first, owner: (own if first else slots.at[owner], slots.at[owner])

    ring = Ring([weight(gate_own, gate_all), weight(up_own, up_all)], ring_send, ring_recv)
    before = {"sp": lax.rem(me + count - 1, count)}
    after = {"sp": lax.rem(me + 1, count)}
    greet([{"sp": ring.next[0]}, {"sp": ring.next[1]}, before, after, partner, *across])

    def halo(which, src, dst):
        return pltpu.make_async_remote_copy(
            src_ref=src.at[length - HALO :],
            dst_ref=dst.at[:HALO],
            send_sem=halo_sem.at[which, 0],
            recv_sem=halo_sem.at[which, 1],
            device_id=after,
            device_id_type=MESH,
        )

    halos = [halo(0, content, padded), halo(1, pairs, map_padded)]

    @pl.when(me < count - 1)
    def _():
        for h in halos:
            h.start()

    ring.start(0, 1)
    ring.start(1, 1)

    @pl.when(me == 0)
    def _():
        padded[:HALO] = jnp.zeros((HALO, channels), padded.dtype)
        map_padded[:HALO] = jnp.zeros((HALO, map_padded.shape[1]), padded.dtype)

    state[...] = jnp.zeros_like(state)
    prior[...] = jnp.zeros_like(prior)
    loads[0].wait()
    loads[1].wait()

    @pl.when(me > 0)
    def _():
        for h in halos:
            h.wait_recv()

    def expand(per_head):
        head = lax.broadcasted_iota(jnp.int32, (heads, channels), 0)
        place = lax.broadcasted_iota(jnp.int32, (heads, channels), 1) // size
        spread = jnp.where(head == place, 1.0, 0.0)
        return dot(per_head, spread, precision=HIGHEST)

    def conv(ref, taps_ref, start, first, width):
        x = ref[pl.ds(start, BLOCK + HALO), first : first + width].astype(jnp.float32)
        total = x[HALO:] * taps_ref[taps - 1 : taps, first : first + width].astype(jnp.float32)
        for tap in range(taps - 1):
            moved = pltpu.roll(x, taps - 1 - tap, 0)[HALO:]
            total += moved * taps_ref[tap : tap + 1, first : first + width].astype(jnp.float32)
        return silu(total).astype(jnp.bfloat16)

    row = lax.broadcasted_iota(jnp.int32, (BLOCK, BLOCK), 0)
    column = lax.broadcasted_iota(jnp.int32, (BLOCK, BLOCK), 1)
    causal = row >= column
    low = column < size

    def block_step(block, _):
        start = pl.multiple_of(block * BLOCK, BLOCK)
        rows = pl.ds(start, BLOCK)
        raised = raw[rows, :].astype(jnp.float32) + shift[...]
        step = jnp.maximum(raised, 0.0) + jnp.log1p(jnp.exp(-jnp.abs(raised)))
        log_decay = -jnp.exp(fading[...]) * step + spike[rows, :]
        cum = dot(jnp.where(causal, 1.0, 0.0), log_decay, precision=HIGHEST)
        end = cum[BLOCK - 1 : BLOCK, :]
        cum_rows = jnp.transpose(cum)
        step_rows = jnp.transpose(step)
        reach[rows, :] = jnp.exp(cum + prior[0:1, :])
        scale = expand(step * jnp.exp(end - cum))
        grow = expand(jnp.exp(cum))
        small = jnp.concatenate(
            [jnp.exp(end), skip[...], jnp.zeros((6, heads), jnp.float32)], axis=0
        )
        small = expand(small)
        keep, direct = small[0:1], small[1:2]
        prior[...] += end
        for group in range(groups):
            maps = conv(map_padded, map_taps, start, group * 2 * BLOCK, 2 * BLOCK)
            write, read = maps[:, :BLOCK], maps[:, BLOCK:]
            read_maps[rows, group * BLOCK : (group + 1) * BLOCK] = read
            inter = dot(read, write, ((1,), (1,)))
            first = group * wide
            held = state[:, first : first + wide]
            carried = dot(read, held.astype(jnp.bfloat16))
            parts = []
            for pair in range(per_group // 2):
                place = first + pair * 2 * size
                value = conv(padded, value_taps, start, place, 2 * size)
                sides = []
                for side in range(2):
                    h = group * per_group + 2 * pair + side
                    gap = cum[:, h : h + 1] - cum_rows[h : h + 1, :]
                    sides.append(
                        (
                            inter
                            * jnp.exp(jnp.where(causal, gap, -1e30))
                            * step_rows[h : h + 1, :]
                        ).astype(jnp.bfloat16)
                    )
                zero = jnp.zeros_like(value)
                stacked = jnp.concatenate(
                    [jnp.where(low, value, zero), jnp.where(low, zero, value)], axis=0
                )
                within = dot(jnp.concatenate(sides, axis=1), stacked)
                value = value.astype(jnp.float32)
                span = slice(place, place + 2 * size)
                local = slice(pair * 2 * size, (pair + 1) * 2 * size)
                mixer[rows, span] = (
                    within + carried[:, local] * grow[:, span] + direct[:, span] * value
                )
                parts.append((value * scale[:, span]).astype(jnp.bfloat16))
            scaled = jnp.concatenate(parts, axis=1)
            added = dot(write, scaled, ((0,), (0,)))
            state[:, first : first + wide] = held * keep[:, first : first + wide] + added
        return 0

    lax.fori_loop(0, blocks, block_step, 0)

    total = expand(prior[...])[0:1]
    upper = total.astype(jnp.bfloat16)
    rest = total - upper.astype(jnp.float32)
    middle = rest.astype(jnp.bfloat16)
    lower = (rest - middle.astype(jnp.float32)).astype(jnp.bfloat16)
    messages[me, :BLOCK] = state[...].astype(jnp.bfloat16)
    messages[me, BLOCK:] = jnp.concatenate(
        [upper, middle, lower, jnp.zeros((HALO - 3, channels), jnp.bfloat16)], axis=0
    )

    def message(part):
        span = pl.ds(part * (channels // 2), channels // 2)

        def refs(first, owner):
            return messages.at[owner, :, span], messages.at[owner, :, span]

        return refs

    scan = Ring([message(0), message(1)], state_send, state_recv)
    for part in range(2):
        scan.start(part, 1)
    for hop in range(2, scan.hops + 1):
        for part in range(2):
            scan.forward(part, hop)
    for piece in range(2):
        ring.forward(piece, 2)
    for part in range(2):
        scan.arrive(part, scan.hops)

    incoming = jnp.zeros((BLOCK, channels), jnp.float32)
    log = jnp.zeros((1, channels), jnp.float32)
    for device in reversed(range(count - 1)):
        counts = jnp.full((1, channels), device, jnp.int32) < me
        theirs = messages[device, :BLOCK].astype(jnp.float32)
        logs = messages[device, BLOCK:].astype(jnp.float32)
        incoming += jnp.where(counts, theirs * jnp.exp(log), 0.0)
        log += jnp.where(counts, logs[0:1] + logs[1:2] + logs[2:3], 0.0)
    state[...] = incoming

    loads[2].wait()
    loads[3].wait()
    blend_width = blend.shape[1]
    pace = 512 if blend_width % 512 == 0 else blend_width

    def project(side, j):
        turn = (core + 1 + side) % CORES
        start = pl.multiple_of(turn * half + j * BLOCK, BLOCK)
        rows = pl.ds(start, BLOCK)
        grow = expand(reach[rows, :])
        for group in range(groups):
            span = slice(group * wide, (group + 1) * wide)
            read = read_maps[rows, group * BLOCK : (group + 1) * BLOCK]
            more = dot(read, state[:, span].astype(jnp.bfloat16)) * grow[:, span]
            gated = (mixer[rows, span] + more) * silu(leave[rows, span].astype(jnp.float32))
            mean = jnp.mean(gated * gated, axis=1, keepdims=True)
            mixed[:, span] = (gated * lax.rsqrt(mean + EPS) * rescale[:, span]).astype(jnp.bfloat16)
        for first in range(0, blend_width, pace):
            partial[side, j, :, first : first + pace] = dot(
                mixed[...], blend[:, first : first + pace]
            ).astype(jnp.bfloat16)

    def to_partner(j):
        return pltpu.make_async_remote_copy(
            src_ref=partial.at[0, j],
            dst_ref=from_partner.at[j],
            send_sem=core_sem.at[0, j],
            recv_sem=core_sem.at[1, j],
            device_id=partner,
            device_id_type=MESH,
        )

    def to_across(s, j):
        return pltpu.make_async_remote_copy(
            src_ref=partial.at[1, j],
            dst_ref=from_across.at[s, j],
            send_sem=across_sem.at[0, s, j],
            recv_sem=across_sem.at[1, s, j],
            device_id=across[s],
            device_id_type=MESH,
        )

    def mid_rows(j):
        return pl.ds(pl.multiple_of(core * half + j * BLOCK, BLOCK), BLOCK)

    def share_mid(j):
        return pltpu.make_async_remote_copy(
            src_ref=mid.at[mid_rows(j)],
            dst_ref=mid.at[mid_rows(j)],
            send_sem=mid_sem.at[0, j],
            recv_sem=mid_sem.at[1, j],
            device_id=partner,
            device_id_type=MESH,
        )

    half_blocks = half // BLOCK

    def exchange_step(j, _):
        project(0, j)
        to_partner(j).start()
        project(1, j)
        to_partner(j).wait_recv()
        partial[1, j] = (
            partial[1, j].astype(jnp.float32) + from_partner[j].astype(jnp.float32)
        ).astype(jnp.bfloat16)
        for s in range(len(across)):
            to_across(s, j).start()
        return 0

    def collect_step(j, _):
        total = partial[1, j].astype(jnp.float32)
        for s in range(len(across)):
            to_across(s, j).wait_recv()
            total += from_across[s, j].astype(jnp.float32)
        own = arrived[pl.ds(pl.multiple_of(j * BLOCK, BLOCK), BLOCK)].astype(jnp.float32)
        mid[mid_rows(j)] = (own + total).astype(jnp.bfloat16)
        share_mid(j).start()
        return 0

    lax.fori_loop(0, half_blocks // 2, exchange_step, 0)
    if ring.hops >= 3:
        ring.forward(0, 3)
    lax.fori_loop(half_blocks // 2, half_blocks, exchange_step, 0)
    if ring.hops >= 3:
        ring.forward(1, 3)
    loads[4].wait()
    lax.fori_loop(0, half_blocks // 2, collect_step, 0)
    for hop in range(4, ring.hops):
        for piece in range(2):
            ring.forward(piece, hop)
    if ring.hops >= 4:
        ring.forward(0, ring.hops)
    lax.fori_loop(half_blocks // 2, half_blocks, collect_step, 0)
    if ring.hops >= 4:
        ring.forward(1, ring.hops)
    for j in range(half_blocks):
        share_mid(j).wait_recv()
    out = pltpu.make_async_copy(mid, mid_out, out_sem)
    out.start()
    for j in range(half_blocks):
        to_partner(j).wait_send()
        share_mid(j).wait_send()
        for s in range(len(across)):
            to_across(s, j).wait_send()
    scan.drain()

    @pl.when(me < count - 1)
    def _():
        for h in halos:
            h.wait_send()

    for piece in range(2):
        ring.arrive(piece, ring.hops)
    ring.drain()
    out.wait()


def feed_kernel(
    mid_hbm, gain, gate_own, up_own, down_own, gate_all, up_all,
    out,
    mid, normed, gate, up, hidden, down, made, from_partner, from_across,
    local_sem, gate_sem, up_sem, ring_send, ring_recv, core_sem, across_sem,
):
    length, width = mid.shape
    count = lax.axis_size("sp")
    me = lax.axis_index("sp")
    tp = lax.axis_index("tp")
    per_tp = count // lax.axis_size("tp")
    chip, core, partner, across = peers()
    chips = len(across) + 1
    depth = gate_own.shape[0]
    units, cut = down_own.shape
    part_units = units // 2

    first_load = pltpu.make_async_copy(mid_hbm, mid, local_sem.at[0])
    first_load.start()

    def load(device, own, slots, into, sem):
        rows = into.at[device * depth : (device + 1) * depth]

        @pl.when(me == device)
        def _():
            pltpu.make_async_copy(own, rows, sem.at[device]).start()

        @pl.when(me != device)
        def _():
            pltpu.make_async_copy(slots.at[device], rows, sem.at[device]).start()

    for device in range(count):
        load(device, gate_own, gate_all, gate, gate_sem)
        load(device, up_own, up_all, up, up_sem)
    own_down = pltpu.make_async_copy(down_own, down.at[me], local_sem.at[1])
    own_down.start()

    def piece(part):
        rows = pl.ds(part * part_units, part_units)

        def refs(first, owner):
            return (
                down_own.at[rows] if first else down.at[owner, rows],
                down.at[owner, rows],
            )

        return refs

    ring = Ring([piece(0), piece(1)], ring_send, ring_recv)
    greet([{"sp": ring.next[0]}, {"sp": ring.next[1]}, partner, *across])
    for part in range(2):
        ring.start(part, 1)

    first_load.wait()

    def norm_step(block, _):
        rows = pl.ds(pl.multiple_of(block * BLOCK, BLOCK), BLOCK)
        x = mid[rows, :].astype(jnp.float32)
        mean = jnp.mean(x * x, axis=1, keepdims=True)
        normed[rows, :] = (x * lax.rsqrt(mean + EPS) * gain[...]).astype(jnp.bfloat16)
        return 0

    lax.fori_loop(0, length // BLOCK, norm_step, 0)
    for device in range(count):
        rows = slice(device * depth, (device + 1) * depth)
        pltpu.make_async_copy(gate_own, gate.at[rows], gate_sem.at[device]).wait()
        pltpu.make_async_copy(up_own, up.at[rows], up_sem.at[device]).wait()
    own_down.wait()

    tall = 256

    def hidden_step(tile, _):
        rows = pl.ds(pl.multiple_of(tile * tall, tall), tall)
        x = normed[rows, :]
        hidden[rows, :] = (silu(dot(x, gate[...])) * dot(x, up[...])).astype(jnp.bfloat16)
        return 0

    tiles = length // tall
    lax.fori_loop(0, tiles // 4, hidden_step, 0)
    ring.forward(0, 2)
    lax.fori_loop(tiles // 4, 3 * tiles // 4, hidden_step, 0)
    ring.forward(1, 2)
    lax.fori_loop(3 * tiles // 4, tiles, hidden_step, 0)

    order = [(me, 0)]
    for hop in range(1, ring.hops + 1):
        order.append((ring.owner(0, hop), hop))
        if 2 * hop < count:
            order.append((ring.owner(1, hop), hop))

    def target(k):
        goal = order[k][0] // per_tp
        return goal, goal // CORES, goal % CORES

    def over_cores(k):
        return pltpu.make_async_remote_copy(
            src_ref=made.at[k],
            dst_ref=from_partner.at[k],
            send_sem=core_sem.at[0, k],
            recv_sem=core_sem.at[1, k],
            device_id=partner,
            device_id_type=MESH,
        )

    def over_chips(k, s):
        return pltpu.make_async_remote_copy(
            src_ref=made.at[k],
            dst_ref=from_across.at[chips - 2 - s, k],
            send_sem=across_sem.at[0, s, k],
            recv_sem=across_sem.at[1, chips - 2 - s, k],
            device_id=across[s],
            device_id_type=MESH,
        )

    def from_chips(k, s):
        return pltpu.make_async_remote_copy(
            src_ref=made.at[k],
            dst_ref=from_across.at[s, k],
            send_sem=across_sem.at[0, s, k],
            recv_sem=across_sem.at[1, s, k],
            device_id=across[s],
            device_id_type=MESH,
        )

    def make(k):
        def tile_step(tile, _):
            rows = pl.ds(pl.multiple_of(tile * tall, tall), tall)
            made[k, rows, :] = dot(hidden[rows, :], down[order[k][0]]).astype(jnp.bfloat16)
            return 0

        lax.fori_loop(0, tiles, tile_step, 0)

        @pl.when(target(k)[2] != core)
        def _():
            over_cores(k).start()

    def combine(k):
        goal, goal_chip, goal_core = target(k)

        @pl.when(goal_core == core)
        def _():
            over_cores(k).wait_recv()
            made[k] = (
                made[k].astype(jnp.float32) + from_partner[k].astype(jnp.float32)
            ).astype(jnp.bfloat16)
            for s in range(chips - 1):

                @pl.when(goal_chip == lax.rem(chip + s + 1, chips))
                def _():
                    over_chips(k, s).start()

    def finish(k):
        owner = order[k][0]

        @pl.when(target(k)[0] == tp)
        def _():
            total = made[k].astype(jnp.float32)
            for s in range(chips - 1):
                from_chips(k, s).wait_recv()
                total += from_across[s, k].astype(jnp.float32)
            at = pl.ds(pl.multiple_of(owner * cut, cut), cut)
            to = pl.ds(pl.multiple_of(lax.rem(owner, per_tp) * cut, cut), cut)
            out[:, to] = (mid[:, at].astype(jnp.float32) + 0.5 * total).astype(jnp.bfloat16)

    done = 0
    make(0)
    for hop in range(1, ring.hops + 1):
        if hop + 1 <= ring.hops and hop > 1:
            ring.forward(0, hop + 1)
            ring.forward(1, hop + 1)
        elif hop == ring.hops:
            ring.arrive(0, hop)
            ring.arrive(1, hop)
        for k in range(len(order)):
            if order[k][1] == hop:
                make(k)
                combine(k - 1)
                if k >= 3:
                    finish(k - 3)
    last = len(order) - 1
    combine(last)
    for k in range(max(last - 2, 0), last + 1):
        finish(k)
    for k in range(last + 1):
        goal, goal_chip, goal_core = target(k)

        @pl.when(goal_core != core)
        def _():
            over_cores(k).wait_send()

        for s in range(chips - 1):

            @pl.when((goal_core == core) & (goal_chip == lax.rem(chip + s + 1, chips)))
            def _():
                over_chips(k, s).wait_send()

    ring.drain()


def shards(
    arriving, content, leaving, linked, raw, spike, value_taps, map_taps,
    shift, fading, skip, rescale, blend, gain, gate, up, down,
):
    length, channels = content.shape
    heads = raw.shape[1]
    groups, state_size = linked.shape[1], linked.shape[3]
    map_width = groups * 2 * state_size
    width = arriving.shape[1]
    taps = value_taps.shape[0]
    count = lax.axis_size("sp")
    hops = count // 2
    chips = lax.axis_size("tp") // CORES
    half = length // CORES
    half_blocks = half // BLOCK
    depth, units = gate.shape
    cut = down.shape[1]
    anywhere = pl.BlockSpec(memory_space=pl.ANY)
    inside = pl.BlockSpec(memory_space=pltpu.VMEM)
    bf16, f32 = jnp.bfloat16, jnp.float32
    dma = pltpu.SemaphoreType.DMA
    mid, gate_all, up_all = pl.pallas_call(
        mixer_kernel,
        out_shape=(
            jax.ShapeDtypeStruct((length, width), bf16),
            jax.ShapeDtypeStruct((count, depth, units), bf16),
            jax.ShapeDtypeStruct((count, depth, units), bf16),
        ),
        in_specs=[anywhere] * 7 + [inside] * 8,
        out_specs=(anywhere,) * 3,
        scratch_shapes=[
            pltpu.VMEM((HALO + length, channels), bf16),
            pltpu.VMEM((HALO + length, map_width), bf16),
            pltpu.VMEM((length, channels), bf16),
            pltpu.VMEM((channels, width), bf16),
            pltpu.VMEM((half, width), bf16),
            pltpu.VMEM((length, groups * state_size), bf16),
            pltpu.VMEM((length, channels), f32),
            pltpu.VMEM((BLOCK, channels), bf16),
            pltpu.VMEM((state_size, channels), f32),
            pltpu.VMEM((length, heads), f32),
            pltpu.VMEM((8, heads), f32),
            pltpu.VMEM((count, state_size + HALO, channels), bf16),
            pltpu.VMEM((CORES, half_blocks, BLOCK, width), bf16),
            pltpu.VMEM((half_blocks, BLOCK, width), bf16),
            pltpu.VMEM((chips - 1, half_blocks, BLOCK, width), bf16),
            pltpu.VMEM((length, width), bf16),
            dma((5,)),
            dma((2, 2)),
            dma((2, 2, hops)),
            dma((2, 2, hops)),
            dma((2, 2, hops)),
            dma((2, 2, hops)),
            dma((2, half_blocks)),
            dma((2, chips - 1, half_blocks)),
            dma((2, half_blocks)),
            dma(()),
        ],
        compiler_params=pltpu.CompilerParams(
            collective_id=0, has_side_effects=True, vmem_limit_bytes=VMEM_BYTES
        ),
        name="mixer",
    )(
        arriving, content, leaving, linked.reshape(length, map_width), gate, up, blend,
        raw, spike, value_taps, map_taps.reshape(taps, map_width),
        shift[None], fading[None], skip[None], rescale[None],
    )
    return pl.pallas_call(
        feed_kernel,
        out_shape=jax.ShapeDtypeStruct((length, width // lax.axis_size("tp")), bf16),
        in_specs=[anywhere, inside] + [anywhere] * 5,
        out_specs=inside,
        scratch_shapes=[
            pltpu.VMEM((length, width), bf16),
            pltpu.VMEM((length, width), bf16),
            pltpu.VMEM((width, units), bf16),
            pltpu.VMEM((width, units), bf16),
            pltpu.VMEM((length, units), bf16),
            pltpu.VMEM((count, units, cut), bf16),
            pltpu.VMEM((count, length, cut), bf16),
            pltpu.VMEM((count, length, cut), bf16),
            pltpu.VMEM((chips - 1, count, length, cut), bf16),
            dma((2,)),
            dma((count,)),
            dma((count,)),
            dma((2, 2, hops)),
            dma((2, 2, hops)),
            dma((2, count)),
            dma((2, chips - 1, count)),
        ],
        compiler_params=pltpu.CompilerParams(
            collective_id=1, has_side_effects=True, vmem_limit_bytes=VMEM_BYTES
        ),
        name="feed",
    )(mid, gain[None], gate, up, down, gate_all, up_all)


def solution(mesh):
    placed = (
        P("sp", None),
        P("sp", "tp"),
        P("sp", "tp"),
        P("sp", "tp", None, None),
        P("sp", "tp"),
        P("sp", "tp"),
        P(None, "tp"),
        P(None, "tp", None, None),
        P("tp"),
        P("tp"),
        P("tp"),
        P("tp"),
        P("tp", None),
        P(),
        P("sp", "tp"),
        P("sp", "tp"),
        P("tp", "sp"),
    )
    return jax.shard_map(
        shards, mesh=mesh, in_specs=placed, out_specs=P("sp", "tp"), check_vma=False
    )
```

profile of v0, /device:TPU:3, one launch (start us, length us, event | category | flops | bytes accessed | tf_op | source)
XLA Modules:
  0.0 229.6 jit_solution(16822969098859965589)
XLA Ops:
  0.0 1.3 reshape.7.map_taps
  1.3 1.6 copy.18.raw
  2.9 1.8 copy.19.spike
  4.7 2.2 reshape.6.pairs
  7.0 137.5 %mixer.1 = (bf16[1024,2048]{1,0:T(8,128)(2,1)}, bf16[8,256,1408]{2,1,0:T(8,128)(2,1)}, bf16[8,256,1408]{2,1,0:T(8,128)(2,1)}) custom-call(bf16[1024,2048]{1,0:T(8,128)(2,1)} %arriving.1, bf16[1024,1024]{1,0:T(8,128)(2,1)} %content.1, bf16[1024,1024]{1,0:T(8,128)(2,1)} %leaving.1, bf16[1024,512]{1,0:T(8,128)(2,1)} %reshape.6.pairs, ...), custom_call_target="tpu_custom_call" | custom-call | tf_op jit(solution)/shard_map/mixer/pallas_call | solution.py:665
  144.5 82.8 %feed.1 = bf16[1024,512]{1,0:T(8,128)(2,1)} custom-call(bf16[1024,2048]{1,0:T(8,128)(2,1)} %get-tuple-element.8.mid_hbm, f32[1,2048]{1,0:T(1,128)} %bitcast.5, bf16[256,1408]{1,0:T(8,128)(2,1)} %gate_own.3, bf16[256,1408]{1,0:T(8,128)(2,1)} %up_own.3, bf16[1408,256]{1,0:T(8,128)(2,1)} %down_own.1, bf16[8,256,1408]{2,1,0:T(8,128)(2,1)} %get-tuple-element.9.gate_all, ...), custom_call_target="tpu_custom_call" | custom-call | tf_op jit(solution)/shard_map/feed/pallas_call | solution.py:711
  227.3 2.3 copy.21
where the time goes:
time: 230 us
  Pallas kernels  220 us (96%)
  local copies, waits for them, and re-layouts  9.23 us (4%)
    pallas_call x1, Pallas kernels, shards(): pl.pallas_call(mixer_kernel, out_shape=(jax.ShapeDtypeStruct((length, wid...  138 us
    pallas_call x1, Pallas kernels, shards(): pl.pallas_call(feed_kernel, out_shape=jax.ShapeDtypeStruct((length, width...  82.8 us
    unnamed x3, local copies, waits for them, and re-layouts  5.7 us

commit v1 on v0

v1 whole, which is shorter than its diff:
```python
import jax
import jax.numpy as jnp
from jax import lax
from jax.experimental import pallas as pl
from jax.experimental.pallas import tpu as pltpu
from jax.sharding import PartitionSpec as P

BLOCK = 128
CORES = 2
EPS = 1e-06
HALO = 16
HIGHEST = lax.Precision.HIGHEST
MESH = pl.DeviceIdType.MESH
VMEM_BYTES = 64_500_000


def ring_shape(count):
    inner = 1
    while inner * inner * 4 <= count:
        inner *= 2
    outer = count // inner
    if inner == 1 or outer % 2:
        return count, 1
    return outer, inner


def ring_at(spot, count):
    outer, inner = ring_shape(count)
    if inner == 1:
        return spot
    if inner == 2:
        late = spot // outer
        return (1 - late) * spot * 2 + late * (2 * (count - 1 - spot) + 1)
    late = jnp.minimum(spot // outer, 1)
    rest = (spot - outer) * late
    lap, step = rest // (inner - 1), rest % (inner - 1)
    odd = lap % 2
    column = (1 + step) * (1 - odd) + (inner - 1 - step) * odd
    return (1 - late) * spot * inner + late * ((outer - 1 - lap) * inner + column)


def ring_spot(index, count):
    outer, inner = ring_shape(count)
    if inner == 1:
        return index
    plane, column = index // inner, index % inner
    late = jnp.minimum(column, 1)
    lap = outer - 1 - plane
    odd = lap % 2
    step = (column - 1) * (1 - odd) + (inner - 1 - column) * odd
    return (1 - late) * plane + late * (outer + lap * (inner - 1) + step)


PIECES = 4
PARTS = 2
DEPTH = 3


class Flow:
    def __init__(self, sets, send_sem, recv_sem):
        count = lax.axis_size("sp")
        spot = ring_spot(lax.axis_index("sp"), count)
        self.count, self.hops, self.spot = count, count // 2, spot
        self.send_sem, self.recv_sem = send_sem, recv_sem
        self.pieces = [piece for group in sets for piece in group]
        self.next = (
            ring_at(lax.rem(spot + 1, count), count),
            ring_at(lax.rem(spot + count - 1, count), count),
        )
        self.order, self.ends = ([], []), []
        first = 0
        for group in sets:
            for hop in range(1, self.hops + 1):
                for piece in range(first, first + len(group)):
                    for way in range(2):
                        if 2 * hop < count or piece % 2 == way:
                            self.order[way].append((piece, hop))
                self.ends.append(len(self.order[0]))
            first += len(group)
        self.total = len(self.order[0])
        self.pushed = self.pulled = 0

    def owner(self, way, hop):
        shift = self.count - hop if way == 0 else hop
        return ring_at(lax.rem(self.spot + shift, self.count), self.count)

    def copy(self, way, step):
        piece, hop = self.order[way][step]
        src, dst = self.pieces[piece](hop == 1, self.owner(way, hop - 1))
        return pltpu.make_async_remote_copy(
            src_ref=src,
            dst_ref=dst,
            send_sem=self.send_sem.at[piece, way, hop - 1],
            recv_sem=self.recv_sem.at[piece, way, hop - 1],
            device_id={"sp": self.next[way]},
            device_id_type=MESH,
        )

    def push(self):
        if self.pushed < self.total:
            for way in range(2):
                piece, hop = self.order[way][self.pushed]
                while hop > 1 and self.pulled <= self.order[way].index((piece, hop - 1)):
                    self.pull()
            for way in range(2):
                self.copy(way, self.pushed).start()
            self.pushed += 1

    def pull(self):
        if self.pulled < self.total:
            for way in range(2):
                self.copy(way, self.pulled).wait_recv()
            self.pulled += 1

    def step(self, times=1):
        for _ in range(times):
            self.pull()
            self.push()

    def until(self, pulled):
        while self.pulled < pulled:
            self.step()

    def paced(self, index, counts):
        for i, times in enumerate(counts):
            if times:

                @pl.when(index == i)
                def _():
                    self.step(times)

    def drain(self):
        for step in range(self.total):
            for way in range(2):
                self.copy(way, step).wait_send()


def greet(others):
    barrier = pltpu.get_barrier_semaphore()
    for other in others:
        pl.semaphore_signal(barrier, inc=1, device_id=other, device_id_type=MESH)
    pl.semaphore_wait(barrier, len(others))


def peers():
    tp = lax.axis_index("tp")
    chips = lax.axis_size("tp") // CORES
    chip, core = tp // CORES, tp % CORES
    partner = {"tp": chip * CORES + 1 - core}
    across = [{"tp": lax.rem(chip + s, chips) * CORES + core} for s in range(1, chips)]
    return chip, core, partner, across


def silu(x):
    return x / (1.0 + jnp.exp(-x))


def dot(a, b, dims=((1,), (0,)), precision=None):
    return lax.dot_general(
        a, b, (dims, ((), ())), precision=precision, preferred_element_type=jnp.float32
    )


def layer_kernel(
    arriving, content, leaving, pairs, gate_own, up_own, down_own, blend_hbm,
    raw, spike, value_taps, map_taps, shift, fading, skip, rescale, gain,
    out,
    padded, map_padded, regroup, leave, blend, arrived, read_maps, mixer, mixed, state, reach, prior,
    messages, chain, partial, from_partner, from_across, mid, resid,
    gate, up, hidden, down, made, made_partner, made_across,
    local_sem, halo_sem, ring_send, ring_recv, plane_send, plane_recv, chain_sem,
    core_sem, across_sem, mid_sem, made_core_sem, made_across_sem,
):
    length, channels = content.shape
    heads = raw.shape[0]
    size = channels // heads
    groups = read_maps.shape[1] // BLOCK
    wide = channels // groups
    per_group = heads // groups
    taps = value_taps.shape[0]
    kinds = groups * 2
    blocks = length // BLOCK
    half = length // CORES
    half_blocks = half // BLOCK
    count = lax.axis_size("sp")
    me = lax.axis_index("sp")
    tp = lax.axis_index("tp")
    per_tp = count // lax.axis_size("tp")
    chip, core, partner, across = peers()
    chips = len(across) + 1
    depth = gate_own.shape[0]
    planes, inner = ring_shape(count)
    plane, spoke = me // inner, lax.rem(me, inner)
    sides, units = down.shape[1], down.shape[2]

    loads = [
        pltpu.make_async_copy(content, padded.at[HALO:], local_sem.at[0]),
        pltpu.make_async_copy(pairs, map_padded.at[HALO * kinds :], local_sem.at[1]),
        pltpu.make_async_copy(leaving, leave, local_sem.at[2]),
        pltpu.make_async_copy(blend_hbm, blend, local_sem.at[3]),
        pltpu.make_async_copy(
            arriving.at[pl.ds(pl.multiple_of(core * half, half), half)], arrived, local_sem.at[4]
        ),
    ]
    mine = pl.ds(pl.multiple_of(me * depth, depth), depth)
    loads.append(pltpu.make_async_copy(gate_own, gate.at[mine], local_sem.at[5]))
    loads.append(pltpu.make_async_copy(up_own, up.at[mine], local_sem.at[6]))
    for side in range(sides):
        loads.append(
            pltpu.make_async_copy(
                down_own.at[:, pl.ds(side * BLOCK, BLOCK)], down.at[me, side], local_sem.at[7 + side]
            )
        )
    loads[0].start()
    loads[1].start()

    def rows_piece(own, whole, part):
        tall = depth // PIECES

        def refs(first, owner):
            at = pl.multiple_of(owner * depth + part * tall, tall)
            target = whole.at[pl.ds(at, tall)]
            return (own.at[pl.ds(part * tall, tall)] if first else target), target

        return refs

    def down_piece(side, part):
        rows = pl.ds(part * (units // 2), units // 2)

        def refs(first, owner):
            target = down.at[owner, side, rows]
            source = down_own.at[rows, pl.ds(side * BLOCK, BLOCK)]
            return (source if first else target), target

        return refs

    flow = Flow(
        [
            [rows_piece(gate_own, gate, part) for part in range(PIECES)]
            + [rows_piece(up_own, up, part) for part in range(PIECES)],
            [down_piece(side, part) for side in range(sides) for part in range(2)],
        ],
        ring_send,
        ring_recv,
    )
    fed = flow.ends[flow.hops - 1]
    before = {"sp": lax.rem(me + count - 1, count)}
    after = {"sp": lax.rem(me + 1, count)}
    siblings = [{"sp": plane * inner + lax.rem(spoke + s, inner)} for s in range(1, inner)]
    below = {"sp": lax.rem(me + inner, count)}
    above = {"sp": lax.rem(me + count - inner, count)}
    greet(
        [
            {"sp": flow.next[0]}, {"sp": flow.next[1]}, before, after, below, above,
            partner, *across, *siblings,
        ]
    )

    def halo(which, src, dst, rows):
        return pltpu.make_async_remote_copy(
            src_ref=src.at[src.shape[0] - rows :],
            dst_ref=dst.at[:rows],
            send_sem=halo_sem.at[which, 0],
            recv_sem=halo_sem.at[which, 1],
            device_id=after,
            device_id_type=MESH,
        )

    halos = [halo(0, content, padded, HALO), halo(1, pairs, map_padded, HALO * kinds)]

    @pl.when(me < count - 1)
    def _():
        for h in halos:
            h.start()

    for _ in range(DEPTH):
        flow.push()
    for load in loads[2:]:
        load.start()

    @pl.when(me == 0)
    def _():
        padded[:HALO] = jnp.zeros((HALO, channels), padded.dtype)
        map_padded[: HALO * kinds] = jnp.zeros((HALO * kinds, BLOCK), padded.dtype)

    to = lax.broadcasted_iota(jnp.int32, regroup.shape, 0)
    at = lax.broadcasted_iota(jnp.int32, regroup.shape, 1)
    regroup[...] = jnp.where(to == lax.rem(at, kinds) * BLOCK + at // kinds, 1.0, 0.0).astype(
        jnp.bfloat16
    )
    state[...] = jnp.zeros_like(state)
    prior[...] = jnp.zeros_like(prior)
    loads[0].wait()
    loads[1].wait()

    @pl.when(me > 0)
    def _():
        for h in halos:
            h.wait_recv()

    head = lax.broadcasted_iota(jnp.int32, (heads, channels), 0)
    place = lax.broadcasted_iota(jnp.int32, (heads, channels), 1) // size
    spread = jnp.where(head == place, 1.0, 0.0).astype(jnp.bfloat16)
    spread = jnp.concatenate([spread] * 3, axis=0)

    def expand(per_head):
        upper = per_head.astype(jnp.bfloat16)
        rest = per_head - upper.astype(jnp.float32)
        middle = rest.astype(jnp.bfloat16)
        lower = (rest - middle.astype(jnp.float32)).astype(jnp.bfloat16)
        return dot(jnp.concatenate([upper, middle, lower], axis=1), spread)

    def conv(ref, weights, start, first, width):
        x = ref[pl.ds(start, BLOCK + HALO), first : first + width].astype(jnp.float32)
        total = x[HALO:] * weights[taps - 1]
        for tap in range(taps - 1):
            total += pltpu.roll(x, taps - 1 - tap, 0)[HALO:] * weights[tap]
        return silu(total).astype(jnp.bfloat16)

    def map_conv(start):
        tall = BLOCK * kinds
        first = pl.multiple_of(start * kinds, tall)
        x = map_padded[pl.ds(first, tall + HALO * kinds), :].astype(jnp.float32)
        total = jnp.zeros((tall // 8, 8, BLOCK), jnp.float32)
        for tap in range(taps):
            line = [
                map_taps[tap, kind // 2, kind % 2 : kind % 2 + 1, :].astype(jnp.float32)
                for kind in range(kinds)
            ]
            weights = jnp.concatenate(line * (8 // kinds), axis=0)
            moved = x if tap == taps - 1 else pltpu.roll(x, (taps - 1 - tap) * kinds, 0)
            total += moved[HALO * kinds :].reshape(total.shape) * weights[None]
        maps = silu(total).reshape(tall, BLOCK).astype(jnp.bfloat16)
        return dot(regroup[...], maps).astype(jnp.bfloat16)

    row = lax.broadcasted_iota(jnp.int32, (BLOCK, BLOCK), 0)
    column = lax.broadcasted_iota(jnp.int32, (BLOCK, BLOCK), 1)
    causal = row >= column
    low = column < size
    running = jnp.where(row <= column, 1.0, 0.0)
    shift_rows = jnp.transpose(jnp.broadcast_to(shift[...], (BLOCK, heads)))
    rate_rows = jnp.transpose(jnp.broadcast_to(-jnp.exp(fading[...]), (BLOCK, heads)))
    direct = expand(jnp.broadcast_to(skip[...], (8, heads)))[0:1]

    def block_step(block, _):
        start = pl.multiple_of(block * BLOCK, BLOCK)
        rows = pl.ds(start, BLOCK)
        raised = raw[:, rows].astype(jnp.float32) + shift_rows
        step_rows = jnp.maximum(raised, 0.0) + jnp.log1p(jnp.exp(-jnp.abs(raised)))
        log_decay = rate_rows * step_rows + spike[:, rows]
        cum_rows = dot(log_decay, running, precision=HIGHEST)
        end = cum_rows[:, BLOCK - 1 : BLOCK]
        reach[:, rows] = jnp.exp(cum_rows + prior[...])
        prior[...] += jnp.broadcast_to(end, prior.shape)
        columns = jnp.transpose(
            jnp.concatenate(
                [cum_rows, step_rows * jnp.exp(end - cum_rows), jnp.exp(cum_rows)], axis=0
            )
        )
        cum = columns[:, :heads]
        scale = expand(columns[:, heads : 2 * heads])
        grow = expand(columns[:, 2 * heads :])
        keep = grow[BLOCK - 1 : BLOCK]
        maps = map_conv(start)
        for group in range(groups):
            write = maps[2 * group * BLOCK : (2 * group + 1) * BLOCK]
            read = maps[(2 * group + 1) * BLOCK : (2 * group + 2) * BLOCK]
            read_maps[rows, group * BLOCK : (group + 1) * BLOCK] = read
            inter = dot(read, write, ((1,), (1,)))
            first = group * wide
            held = state[:, first : first + wide]
            carried = dot(read, held.astype(jnp.bfloat16))
            parts = []
            for pair in range(per_group // 2):
                place = first + pair * 2 * size
                span = slice(place, place + 2 * size)
                weights = [
                    value_taps[tap : tap + 1, span].astype(jnp.float32) for tap in range(taps)
                ]
                value = conv(padded, weights, start, place, 2 * size)
                sides = []
                for side in range(2):
                    h = group * per_group + 2 * pair + side
                    gap = cum[:, h : h + 1] - cum_rows[h : h + 1, :]
                    sides.append(
                        (
                            inter
                            * jnp.exp(jnp.where(causal, gap, -1e30))
                            * step_rows[h : h + 1, :]
                        ).astype(jnp.bfloat16)
                    )
                zero = jnp.zeros_like(value)
                stacked = jnp.concatenate(
                    [jnp.where(low, value, zero), jnp.where(low, zero, value)], axis=0
                )
                within = dot(jnp.concatenate(sides, axis=1), stacked)
                value = value.astype(jnp.float32)
                local = slice(pair * 2 * size, (pair + 1) * 2 * size)
                mixer[rows, span] = (
                    within + carried[:, local] * grow[:, span] + direct[:, span] * value
                )
                parts.append((value * scale[:, span]).astype(jnp.bfloat16))
            scaled = jnp.concatenate(parts, axis=1)
            added = dot(write, scaled, ((0,), (0,)))
            state[:, first : first + wide] = held * keep[:, first : first + wide] + added
        return 0

    def local_step(turn, _):
        lax.fori_loop(2 * turn, 2 * turn + 2, block_step, 0)
        flow.paced(turn, [0, 1, 1, 1])
        return 0

    lax.fori_loop(0, blocks // 2, local_step, 0)

    total = expand(jnp.transpose(prior[...]))[0:1]
    upper = total.astype(jnp.bfloat16)
    rest = total - upper.astype(jnp.float32)
    middle = rest.astype(jnp.bfloat16)
    lower = (rest - middle.astype(jnp.float32)).astype(jnp.bfloat16)
    messages[spoke, BLOCK:] = jnp.concatenate(
        [upper, middle, lower, jnp.zeros((HALO - 3, channels), jnp.bfloat16)], axis=0
    )
    messages[spoke, :BLOCK] = state[...].astype(jnp.bfloat16)

    def to_sibling(s):
        return pltpu.make_async_remote_copy(
            src_ref=messages.at[spoke],
            dst_ref=messages.at[spoke],
            send_sem=plane_send.at[s],
            recv_sem=plane_recv.at[inner - 2 - s],
            device_id=siblings[s],
            device_id_type=MESH,
        )

    for s in range(inner - 1):
        to_sibling(s).start()
    flow.pull()
    flow.step(2)
    for s in range(inner - 1):
        to_sibling(inner - 2 - s).wait_recv()

    bands = 2
    band = channels // bands

    def pass_on(part):
        span = pl.ds(part * band, band)
        return pltpu.make_async_remote_copy(
            src_ref=chain.at[1, :, span],
            dst_ref=chain.at[0, :, span],
            send_sem=chain_sem.at[0, part],
            recv_sem=chain_sem.at[1, part],
            device_id=below,
            device_id_type=MESH,
        )

    def logs_of(other):
        terms = messages[other, BLOCK:].astype(jnp.float32)
        return terms[0:1] + terms[1:2] + terms[2:3]

    logs = [logs_of(other) for other in range(inner)]

    def plane_sum(part, behind):
        span = slice(part * band, (part + 1) * band)
        summed = jnp.zeros((BLOCK, band), jnp.float32)
        log = jnp.zeros((1, band), jnp.float32)
        for other in reversed(range(inner)):
            theirs = messages[other, :BLOCK, span].astype(jnp.float32) * jnp.exp(log)
            if behind:
                counts = jnp.full((1, band), other, jnp.int32) < spoke
                summed += jnp.where(counts, theirs, 0.0)
                log += jnp.where(counts, logs[other][:, span], 0.0)
            else:
                summed += theirs
                log += logs[other][:, span]
        return summed, jnp.exp(log)

    @pl.when(plane == 0)
    def _():
        chain[0] = jnp.zeros((BLOCK, channels), jnp.bfloat16)
        for part in range(bands):
            chain[1, :, part * band : (part + 1) * band] = plane_sum(part, False)[0].astype(
                jnp.bfloat16
            )
            pass_on(part).start()

    for link in range(planes - 1):
        flow.step(3)

        @pl.when(plane == link + 1)
        def _():
            for part in range(bands):
                span = slice(part * band, (part + 1) * band)
                pass_on(part).wait_recv()
                if link + 2 < planes:
                    summed, decay = plane_sum(part, False)
                    chain[1, :, span] = (
                        chain[0, :, span].astype(jnp.float32) * decay + summed
                    ).astype(jnp.bfloat16)
                    pass_on(part).start()

    for part in range(bands):
        span = slice(part * band, (part + 1) * band)
        summed, decay = plane_sum(part, True)
        state[:, span] = chain[0, :, span].astype(jnp.float32) * decay + summed
    flow.push()

    loads[2].wait()
    loads[3].wait()
    blend_width = blend.shape[1]
    pace = 512 if blend_width % 512 == 0 else blend_width

    def project(side, j):
        turn = (core + 1 + side) % CORES
        start = pl.multiple_of(turn * half + j * BLOCK, BLOCK)
        rows = pl.ds(start, BLOCK)
        grow = expand(jnp.transpose(reach[:, rows]))
        for group in range(groups):
            span = slice(group * wide, (group + 1) * wide)
            read = read_maps[rows, group * BLOCK : (group + 1) * BLOCK]
            more = dot(read, state[:, span].astype(jnp.bfloat16)) * grow[:, span]
            gated = (mixer[rows, span] + more) * silu(leave[rows, span].astype(jnp.float32))
            mean = jnp.mean(gated * gated, axis=1, keepdims=True)
            mixed[:, span] = (gated * lax.rsqrt(mean + EPS) * rescale[:, span]).astype(jnp.bfloat16)
        for first in range(0, blend_width, pace):
            partial[side, j, :, first : first + pace] = dot(
                mixed[...], blend[:, first : first + pace]
            ).astype(jnp.bfloat16)

    def to_partner(j):
        return pltpu.make_async_remote_copy(
            src_ref=partial.at[0, j],
            dst_ref=from_partner.at[j],
            send_sem=core_sem.at[0, j],
            recv_sem=core_sem.at[1, j],
            device_id=partner,
            device_id_type=MESH,
        )

    def to_across(s, j):
        return pltpu.make_async_remote_copy(
            src_ref=partial.at[1, j],
            dst_ref=from_across.at[s, j],
            send_sem=across_sem.at[0, s, j],
            recv_sem=across_sem.at[1, s, j],
            device_id=across[s],
            device_id_type=MESH,
        )

    def mid_rows(j):
        return pl.ds(pl.multiple_of(core * half + j * BLOCK, BLOCK), BLOCK)

    def share_mid(j):
        return pltpu.make_async_remote_copy(
            src_ref=mid.at[mid_rows(j)],
            dst_ref=mid.at[mid_rows(j)],
            send_sem=mid_sem.at[0, j],
            recv_sem=mid_sem.at[1, j],
            device_id=partner,
            device_id_type=MESH,
        )

    def exchange_step(j, _):
        project(0, j)
        to_partner(j).start()
        flow.paced(j, [0, 1, 1, 1])
        project(1, j)
        to_partner(j).wait_recv()
        partial[1, j] = (
            partial[1, j].astype(jnp.float32) + from_partner[j].astype(jnp.float32)
        ).astype(jnp.bfloat16)
        for s in range(len(across)):
            to_across(s, j).start()
        return 0

    def collect_step(j, _):
        flow.paced(j, [1, 3, 3, 3])
        total = partial[1, j].astype(jnp.float32)
        for s in range(len(across)):
            to_across(s, j).wait_recv()
            total += from_across[s, j].astype(jnp.float32)
        own = arrived[pl.ds(pl.multiple_of(j * BLOCK, BLOCK), BLOCK)].astype(jnp.float32)
        mid[mid_rows(j)] = (own + total).astype(jnp.bfloat16)
        share_mid(j).start()
        return 0

    lax.fori_loop(0, half_blocks, exchange_step, 0)
    loads[4].wait()
    lax.fori_loop(0, half_blocks, collect_step, 0)
    for j in range(half_blocks):
        share_mid(j).wait_recv()
        share_mid(j).wait_send()
    own_width = resid.shape[1]

    def norm_step(block, _):
        rows = pl.ds(pl.multiple_of(block * BLOCK, BLOCK), BLOCK)
        resid[rows, :] = mid[rows, pl.ds(pl.multiple_of(tp * own_width, own_width), own_width)]
        x = mid[rows, :].astype(jnp.float32)
        mean = jnp.mean(x * x, axis=1, keepdims=True)
        mid[rows, :] = (x * lax.rsqrt(mean + EPS) * gain[...]).astype(jnp.bfloat16)
        return 0

    lax.fori_loop(0, blocks, norm_step, 0)
    for load in loads[5:]:
        load.wait()
    flow.until(fed)

    tall = 256
    tiles = length // tall

    def hidden_step(tile, _):
        rows = pl.ds(pl.multiple_of(tile * tall, tall), tall)
        x = mid[rows, :]
        hidden[rows, :] = (silu(dot(x, gate[...])) * dot(x, up[...])).astype(jnp.bfloat16)
        flow.paced(tile, [1, 1, 1, 1])
        return 0

    lax.fori_loop(0, tiles, hidden_step, 0)

    order = [(me, 0)]
    for hop in range(1, flow.hops + 1):
        order.append((flow.owner(0, hop), hop))
        if 2 * hop < count:
            order.append((flow.owner(1, hop), hop))

    def target(k):
        goal = order[k][0] // per_tp
        return goal // CORES, goal % CORES

    def slot(k):
        owner = order[k][0]
        return owner // (per_tp * CORES) * per_tp + lax.rem(owner, per_tp)

    long = length // PARTS
    units_of = [(side, part) for side in range(sides) for part in range(PARTS)]

    def over_cores(k, unit):
        return pltpu.make_async_remote_copy(
            src_ref=made.at[k, unit],
            dst_ref=made_partner.at[slot(k), unit],
            send_sem=made_core_sem.at[0, k, unit],
            recv_sem=made_core_sem.at[1, k, unit],
            device_id=partner,
            device_id_type=MESH,
        )

    def over_chips(k, unit, s, into):
        return pltpu.make_async_remote_copy(
            src_ref=made.at[k, unit],
            dst_ref=made_across.at[into, lax.rem(order[k][0], per_tp), unit],
            send_sem=made_across_sem.at[0, s, k, unit],
            recv_sem=made_across_sem.at[1, into, k, unit],
            device_id=across[s],
            device_id_type=MESH,
        )

    def make(k, unit):
        side, part = units_of[unit]
        for first in range(0, long, tall):
            rows = slice(part * long + first, part * long + first + tall)
            made[k, unit, first : first + tall, :] = dot(
                hidden[rows, :], down[order[k][0], side]
            ).astype(jnp.bfloat16)

        @pl.when(target(k)[1] != core)
        def _():
            over_cores(k, unit).start()

    def combine(k, unit):
        goal_chip, goal_core = target(k)

        @pl.when(goal_core == core)
        def _():
            over_cores(k, unit).wait_recv()
            made[k, unit] = (
                made[k, unit].astype(jnp.float32) + made_partner[slot(k), unit].astype(jnp.float32)
            ).astype(jnp.bfloat16)
            for s in range(chips - 1):

                @pl.when(goal_chip == lax.rem(chip + s + 1, chips))
                def _():
                    over_chips(k, unit, s, chips - 2 - s).start()

    def finish(k, unit):
        owner = order[k][0]
        side, part = units_of[unit]

        @pl.when(owner // per_tp == tp)
        def _():
            total = made[k, unit].astype(jnp.float32)
            for s in range(chips - 1):
                over_chips(k, unit, s, s).wait_recv()
                total += made_across[s, lax.rem(owner, per_tp), unit].astype(jnp.float32)
            at = (lax.rem(owner, per_tp) * sides + side) * BLOCK
            to = pl.ds(pl.multiple_of(at, BLOCK), BLOCK)
            rows = slice(part * long, (part + 1) * long)
            out[rows, to] = (resid[rows, to].astype(jnp.float32) + 0.5 * total).astype(jnp.bfloat16)

    made_units, summed_units, finished = [], 0, 0

    def sum_up_to(n):
        nonlocal summed_units
        while summed_units < n:
            combine(*made_units[summed_units])
            summed_units += 1

    def finish_up_to(n):
        nonlocal finished
        while finished < n:
            finish(*made_units[finished])
            finished += 1

    def handle(ks, side, lag):
        for k in ks:
            for part in range(PARTS):
                make(k, side * PARTS + part)
                made_units.append((k, side * PARTS + part))
                sum_up_to(len(made_units) - lag)

    lag = 3
    for side in range(sides):
        handle([0], side, lag)
    flow.step()
    for hop in range(1, flow.hops + 1):
        ks = [k for k in range(len(order)) if order[k][1] == hop]
        begin, end = flow.ends[flow.hops + hop - 2], flow.ends[flow.hops + hop - 1]
        old = len(made_units)
        for side in range(sides):
            flow.until(begin + (end - begin) * (side + 1) // sides)
            handle(ks, side, lag)
            if 2 * hop < flow.hops:
                flow.step()
            if hop > 1:
                sum_up_to(len(made_units))
        if hop < flow.hops:
            finish_up_to(old)
    finish_up_to(len(made_units))

    @pl.when(me < count - 1)
    def _():
        for h in halos:
            h.wait_send()

    for s in range(inner - 1):
        to_sibling(s).wait_send()

    @pl.when(plane < planes - 1)
    def _():
        for part in range(bands):
            pass_on(part).wait_send()

    for j in range(half_blocks):
        to_partner(j).wait_send()
        for s in range(len(across)):
            to_across(s, j).wait_send()
    flow.drain()
    for k in range(len(order)):
        goal_chip, goal_core = target(k)

        @pl.when(goal_core != core)
        def _():
            for unit in range(len(units_of)):
                over_cores(k, unit).wait_send()

        for s in range(chips - 1):

            @pl.when((goal_core == core) & (goal_chip == lax.rem(chip + s + 1, chips)))
            def _():
                for unit in range(len(units_of)):
                    over_chips(k, unit, s, chips - 2 - s).wait_send()


def shards(
    arriving, content, leaving, linked, raw, spike, value_taps, map_taps,
    shift, fading, skip, rescale, blend, gain, gate, up, down,
):
    length, channels = content.shape
    heads = raw.shape[1]
    groups, state_size = linked.shape[1], linked.shape[3]
    kinds = groups * 2
    width = arriving.shape[1]
    count = lax.axis_size("sp")
    hops = count // 2
    inner = ring_shape(count)[1]
    tp_count = lax.axis_size("tp")
    chips = tp_count // CORES
    half = length // CORES
    half_blocks = half // BLOCK
    units, cut = down.shape
    sides = cut // BLOCK
    per_tp = count // tp_count
    subs = sides * PARTS
    pieces = 2 * PIECES + 2 * sides
    anywhere = pl.BlockSpec(memory_space=pl.ANY)
    inside = pl.BlockSpec(memory_space=pltpu.VMEM)
    bf16, f32 = jnp.bfloat16, jnp.float32
    dma = pltpu.SemaphoreType.DMA
    return pl.pallas_call(
        layer_kernel,
        out_shape=pltpu.VMEM((length, width // tp_count), bf16),
        in_specs=[anywhere] * 8 + [inside] * 9,
        out_specs=inside,
        scratch_shapes=[
            pltpu.VMEM((HALO + length, channels), bf16),
            pltpu.VMEM(((HALO + length) * kinds, state_size), bf16),
            pltpu.VMEM((BLOCK * kinds, BLOCK * kinds), bf16),
            pltpu.VMEM((length, channels), bf16),
            pltpu.VMEM((channels, width), bf16),
            pltpu.VMEM((half, width), bf16),
            pltpu.VMEM((length, groups * state_size), bf16),
            pltpu.VMEM((length, channels), f32),
            pltpu.VMEM((BLOCK, channels), bf16),
            pltpu.VMEM((state_size, channels), f32),
            pltpu.VMEM((heads, length), f32),
            pltpu.VMEM((heads, BLOCK), f32),
            pltpu.VMEM((inner, state_size + HALO, channels), bf16),
            pltpu.VMEM((2, state_size, channels), bf16),
            pltpu.VMEM((CORES, half_blocks, BLOCK, width), bf16),
            pltpu.VMEM((half_blocks, BLOCK, width), bf16),
            pltpu.VMEM((chips - 1, half_blocks, BLOCK, width), bf16),
            pltpu.VMEM((length, width), bf16),
            pltpu.VMEM((length, width // tp_count), bf16),
            pltpu.VMEM((width, units), bf16),
            pltpu.VMEM((width, units), bf16),
            pltpu.VMEM((length, units), bf16),
            pltpu.VMEM((count, sides, units, BLOCK), bf16),
            pltpu.VMEM((count, subs, length // PARTS, BLOCK), bf16),
            pltpu.VMEM((chips * per_tp, subs, length // PARTS, BLOCK), bf16),
            pltpu.VMEM((chips - 1, per_tp, subs, length // PARTS, BLOCK), bf16),
            dma((7 + sides,)),
            dma((2, 2)),
            dma((pieces, 2, hops)),
            dma((pieces, 2, hops)),
            dma((max(inner - 1, 1),)),
            dma((max(inner - 1, 1),)),
            dma((2, 2)),
            dma((2, half_blocks)),
            dma((2, chips - 1, half_blocks)),
            dma((2, half_blocks)),
            dma((2, count, subs)),
            dma((2, chips - 1, count, subs)),
        ],
        compiler_params=pltpu.CompilerParams(
            collective_id=0, has_side_effects=True, vmem_limit_bytes=VMEM_BYTES
        ),
        name="layer",
    )(
        arriving, content, leaving, linked.reshape(length * kinds, state_size), gate, up, down, blend,
        raw.T, spike.T, value_taps, map_taps,
        shift[None], fading[None], skip[None], rescale[None], gain[None],
    )


def solution(mesh):
    placed = (
        P("sp", None),
        P("sp", "tp"),
        P("sp", "tp"),
        P("sp", "tp", None, None),
        P("sp", "tp"),
        P("sp", "tp"),
        P(None, "tp"),
        P(None, "tp", None, None),
        P("tp"),
        P("tp"),
        P("tp"),
        P("tp"),
        P("tp", None),
        P(),
        P("sp", "tp"),
        P("sp", "tp"),
        P("tp", "sp"),
    )
    return jax.shard_map(
        shards, mesh=mesh, in_specs=placed, out_specs=P("sp", "tp"), check_vma=False
    )
```

time: 230 us -> 195 us (0.85); the launches traced: 230 us -> 191 us
  Pallas kernels: 220 us -> 190 us
  local copies, waits for them, and re-layouts: 9.23 us -> 0.97 us
    pallas_call x2 -> x1, Pallas kernels: 220 us -> 190 us  [shards(): pl.pallas_call(layer_kernel, out_shape=pltpu.VMEM((length, width // tp_co...]
    unnamed x3 -> x1, local copies, waits for them, and re-layouts: 5.7 us -> 0.97 us
    reshape x2 -> x0, local copies, waits for them, and re-layouts: 3.53 us -> none  [the longest x1 2.24 us: shards(): linked.reshape(length, map_width)]
where the time goes in v1:
time: 195 us; the launch traced here: 191 us
  Pallas kernels  190 us (97%)
    pallas_call x1, Pallas kernels, shards(): pl.pallas_call(layer_kernel, out_shape=pltpu.VMEM((length, width // tp_co...  190 us

profile of v1, /device:TPU:3, one launch (start us, length us, event | category | flops | bytes accessed | tf_op | source)
XLA Modules:
  0.0 191.5 jit_solution(16862855950084728711)
XLA Ops:
  0.0 190.5 %layer.1 = bf16[1024,512]{1,0:T(8,128)(2,1)S(1)} custom-call(bf16[1024,2048]{1,0:T(8,128)(2,1)} %arriving.1, bf16[1024,1024]{1,0:T(8,128)(2,1)} %content.1, bf16[1024,1024]{1,0:T(8,128)(2,1)} %leaving.1, bf16[4096,128]{1,0:T(8,128)(2,1)} %bitcast.8, bf16[256,1408]{1,0:T(8,128)(2,1)} %gate_own.1, bf16[256,1408]{1,0:T(8,128)(2,1)} %up_own.1, ...), custom_call_target="tpu_custom_call" | custom-call | tf_op jit(solution)/shard_map/layer/pallas_call | solution.py:797
  190.5 1.0 copy.19

commit v2 on v1

--- a/solution.py
+++ b/solution.py
@@ -11,7 +11,7 @@
 HALO = 16
 HIGHEST = lax.Precision.HIGHEST
 MESH = pl.DeviceIdType.MESH
-VMEM_BYTES = 64_500_000
+VMEM_BYTES = 65_500_000
 
 
 def ring_shape(count):
@@ -53,6 +53,7 @@
 
 PIECES = 4
 PARTS = 2
+SLOTS = 8
 DEPTH = 3
 
 
@@ -90,8 +91,8 @@
         return pltpu.make_async_remote_copy(
             src_ref=src,
             dst_ref=dst,
-            send_sem=self.send_sem.at[piece, way, hop - 1],
-            recv_sem=self.recv_sem.at[piece, way, hop - 1],
+            send_sem=self.send_sem.at[way, step % SLOTS],
+            recv_sem=self.recv_sem.at[way, step % SLOTS],
             device_id={"sp": self.next[way]},
             device_id_type=MESH,
         )
@@ -103,6 +104,8 @@
                 while hop > 1 and self.pulled <= self.order[way].index((piece, hop - 1)):
                     self.pull()
             for way in range(2):
+                if self.pushed >= SLOTS:
+                    self.copy(way, self.pushed - SLOTS).wait_send()
                 self.copy(way, self.pushed).start()
             self.pushed += 1
 
@@ -130,7 +133,7 @@
                     self.step(times)
 
     def drain(self):
-        for step in range(self.total):
+        for step in range(max(self.total - SLOTS, 0), self.total):
             for way in range(2):
                 self.copy(way, step).wait_send()
 
@@ -165,7 +168,8 @@
     arriving, content, leaving, pairs, gate_own, up_own, down_own, blend_hbm,
     raw, spike, value_taps, map_taps, shift, fading, skip, rescale, gain,
     out,
-    padded, map_padded, regroup, leave, blend, arrived, read_maps, mixer, mixed, state, reach, prior,
+    padded, map_padded, regroup, leave, blend, arrived, entering, mixer, mixed, state,
+    cums, steps, reach, prior,
     messages, chain, partial, from_partner, from_across, mid, resid,
     gate, up, hidden, down, made, made_partner, made_across,
     local_sem, halo_sem, ring_send, ring_recv, plane_send, plane_recv, chain_sem,
@@ -174,7 +178,7 @@
     length, channels = content.shape
     heads = raw.shape[0]
     size = channels // heads
-    groups = read_maps.shape[1] // BLOCK
+    groups = map_taps.shape[1]
     wide = channels // groups
     per_group = heads // groups
     taps = value_taps.shape[0]
@@ -342,7 +346,10 @@
     rate_rows = jnp.transpose(jnp.broadcast_to(-jnp.exp(fading[...]), (BLOCK, heads)))
     direct = expand(jnp.broadcast_to(skip[...], (8, heads)))[0:1]
 
-    def block_step(block, _):
+    def map_rows(start, kind):
+        return pl.ds(pl.multiple_of(start * kinds, BLOCK) + kind * BLOCK, BLOCK)
+
+    def state_step(block, _):
         start = pl.multiple_of(block * BLOCK, BLOCK)
         rows = pl.ds(start, BLOCK)
         raised = raw[:, rows].astype(jnp.float32) + shift_rows
@@ -350,39 +357,58 @@
         log_decay = rate_rows * step_rows + spike[:, rows]
         cum_rows = dot(log_decay, running, precision=HIGHEST)
         end = cum_rows[:, BLOCK - 1 : BLOCK]
+        cums[:, rows] = cum_rows
+        steps[:, rows] = step_rows
         reach[:, rows] = jnp.exp(cum_rows + prior[...])
         prior[...] += jnp.broadcast_to(end, prior.shape)
         columns = jnp.transpose(
-            jnp.concatenate(
-                [cum_rows, step_rows * jnp.exp(end - cum_rows), jnp.exp(cum_rows)], axis=0
-            )
-        )
-        cum = columns[:, :heads]
-        scale = expand(columns[:, heads : 2 * heads])
-        grow = expand(columns[:, 2 * heads :])
-        keep = grow[BLOCK - 1 : BLOCK]
+            jnp.concatenate([step_rows * jnp.exp(end - cum_rows), jnp.exp(cum_rows)], axis=0)
+        )
+        scale = expand(columns[:, :heads])
+        keep = expand(columns[BLOCK - 8 :, heads:])[7:8]
         maps = map_conv(start)
+        map_padded[pl.ds(pl.multiple_of(start * kinds, BLOCK), BLOCK * kinds), :] = maps
+        entering[block] = state[...].astype(jnp.bfloat16)
         for group in range(groups):
             write = maps[2 * group * BLOCK : (2 * group + 1) * BLOCK]
-            read = maps[(2 * group + 1) * BLOCK : (2 * group + 2) * BLOCK]
-            read_maps[rows, group * BLOCK : (group + 1) * BLOCK] = read
+            first = group * wide
+            parts = []
+            for place in range(first, first + wide, BLOCK):
+                span = slice(place, place + BLOCK)
+                weights = [
+                    value_taps[tap : tap + 1, span].astype(jnp.float32) for tap in range(taps)
+                ]
+                value = conv(padded, weights, start, place, BLOCK)
+                padded[rows, span] = value
+                parts.append((value.astype(jnp.float32) * scale[:, span]).astype(jnp.bfloat16))
+            span = slice(first, first + wide)
+            added = dot(write, jnp.concatenate(parts, axis=1), ((0,), (0,)))
+            state[:, span] = state[:, span] * keep[:, span] + added
+        return 0
+
+    def block_step(block, _):
+        start = pl.multiple_of(block * BLOCK, BLOCK)
+        rows = pl.ds(start, BLOCK)
+        cum_rows = cums[:, rows]
+        step_rows = steps[:, rows]
+        columns = jnp.transpose(jnp.concatenate([cum_rows, jnp.exp(cum_rows)], axis=0))
+        cum = columns[:, :heads]
+        grow = expand(columns[:, heads:])
+        for group in range(groups):
+            write = map_padded[map_rows(start, 2 * group), :]
+            read = map_padded[map_rows(start, 2 * group + 1), :]
             inter = dot(read, write, ((1,), (1,)))
             first = group * wide
-            held = state[:, first : first + wide]
-            carried = dot(read, held.astype(jnp.bfloat16))
-            parts = []
+            carried = dot(read, entering[block, :, first : first + wide])
             for pair in range(per_group // 2):
                 place = first + pair * 2 * size
                 span = slice(place, place + 2 * size)
-                weights = [
-                    value_taps[tap : tap + 1, span].astype(jnp.float32) for tap in range(taps)
-                ]
-                value = conv(padded, weights, start, place, 2 * size)
-                sides = []
+                value = padded[rows, span]
+                sides_ = []
                 for side in range(2):
                     h = group * per_group + 2 * pair + side
                     gap = cum[:, h : h + 1] - cum_rows[h : h + 1, :]
-                    sides.append(
+                    sides_.append(
                         (
                             inter
                             * jnp.exp(jnp.where(causal, gap, -1e30))
@@ -393,21 +419,18 @@
                 stacked = jnp.concatenate(
                     [jnp.where(low, value, zero), jnp.where(low, zero, value)], axis=0
                 )
-                within = dot(jnp.concatenate(sides, axis=1), stacked)
-                value = value.astype(jnp.float32)
+                within = dot(jnp.concatenate(sides_, axis=1), stacked)
                 local = slice(pair * 2 * size, (pair + 1) * 2 * size)
                 mixer[rows, span] = (
-                    within + carried[:, local] * grow[:, span] + direct[:, span] * value
+                    within
+                    + carried[:, local] * grow[:, span]
+                    + direct[:, span] * value.astype(jnp.float32)
                 )
-                parts.append((value * scale[:, span]).astype(jnp.bfloat16))
-            scaled = jnp.concatenate(parts, axis=1)
-            added = dot(write, scaled, ((0,), (0,)))
-            state[:, first : first + wide] = held * keep[:, first : first + wide] + added
         return 0
 
     def local_step(turn, _):
-        lax.fori_loop(2 * turn, 2 * turn + 2, block_step, 0)
-        flow.paced(turn, [0, 1, 1, 1])
+        lax.fori_loop(2 * turn, 2 * turn + 2, state_step, 0)
+        flow.paced(turn, [0, 0, 0, 1])
         return 0
 
     lax.fori_loop(0, blocks // 2, local_step, 0)
@@ -434,10 +457,6 @@
 
     for s in range(inner - 1):
         to_sibling(s).start()
-    flow.pull()
-    flow.step(2)
-    for s in range(inner - 1):
-        to_sibling(inner - 2 - s).wait_recv()
 
     bands = 2
     band = channels // bands
@@ -457,10 +476,9 @@
         terms = messages[other, BLOCK:].astype(jnp.float32)
         return terms[0:1] + terms[1:2] + terms[2:3]
 
-    logs = [logs_of(other) for other in range(inner)]
-
     def plane_sum(part, behind):
         span = slice(part * band, (part + 1) * band)
+        logs = [logs_of(other) for other in range(inner)]
         summed = jnp.zeros((BLOCK, band), jnp.float32)
         log = jnp.zeros((1, band), jnp.float32)
         for other in reversed(range(inner)):
@@ -474,18 +492,20 @@
                 log += logs[other][:, span]
         return summed, jnp.exp(log)
 
-    @pl.when(plane == 0)
-    def _():
-        chain[0] = jnp.zeros((BLOCK, channels), jnp.bfloat16)
-        for part in range(bands):
-            chain[1, :, part * band : (part + 1) * band] = plane_sum(part, False)[0].astype(
-                jnp.bfloat16
-            )
-            pass_on(part).start()
-
-    for link in range(planes - 1):
-        flow.step(3)
-
+    def begin_chain():
+        for s in range(inner - 1):
+            to_sibling(inner - 2 - s).wait_recv()
+
+        @pl.when(plane == 0)
+        def _():
+            chain[0] = jnp.zeros((BLOCK, channels), jnp.bfloat16)
+            for part in range(bands):
+                chain[1, :, part * band : (part + 1) * band] = plane_sum(part, False)[0].astype(
+                    jnp.bfloat16
+                )
+                pass_on(part).start()
+
+    def join_chain(link):
         @pl.when(plane == link + 1)
         def _():
             for part in range(bands):
@@ -498,11 +518,33 @@
                     ).astype(jnp.bfloat16)
                     pass_on(part).start()
 
+    turns = blocks // 2
+
+    def scan_step(turn, _):
+        lax.fori_loop(2 * turn, 2 * turn + 2, block_step, 0)
+        flow.paced(turn, [1, 2] + [3] * (turns - 2))
+
+        @pl.when(turn == 1)
+        def _():
+            begin_chain()
+
+        for link in range(min(turns - 2, planes - 1)):
+
+            @pl.when(turn == link + 2)
+            def _():
+                join_chain(link)
+
+        return 0
+
+    lax.fori_loop(0, turns, scan_step, 0)
+    for link in range(turns - 2, planes - 1):
+        flow.step(3)
+        join_chain(link)
+
     for part in range(bands):
         span = slice(part * band, (part + 1) * band)
         summed, decay = plane_sum(part, True)
         state[:, span] = chain[0, :, span].astype(jnp.float32) * decay + summed
-    flow.push()
 
     loads[2].wait()
     loads[3].wait()
@@ -516,7 +558,7 @@
         grow = expand(jnp.transpose(reach[:, rows]))
         for group in range(groups):
             span = slice(group * wide, (group + 1) * wide)
-            read = read_maps[rows, group * BLOCK : (group + 1) * BLOCK]
+            read = map_padded[map_rows(start, 2 * group + 1), :]
             more = dot(read, state[:, span].astype(jnp.bfloat16)) * grow[:, span]
             gated = (mixer[rows, span] + more) * silu(leave[rows, span].astype(jnp.float32))
             mean = jnp.mean(gated * gated, axis=1, keepdims=True)
@@ -726,7 +768,7 @@
         old = len(made_units)
         for side in range(sides):
             flow.until(begin + (end - begin) * (side + 1) // sides)
-            handle(ks, side, lag)
+            handle(ks, side, lag if hop < 3 else 2)
             if 2 * hop < flow.hops:
                 flow.step()
             if hop > 1:
@@ -779,7 +821,6 @@
     kinds = groups * 2
     width = arriving.shape[1]
     count = lax.axis_size("sp")
-    hops = count // 2
     inner = ring_shape(count)[1]
     tp_count = lax.axis_size("tp")
     chips = tp_count // CORES
@@ -789,7 +830,6 @@
     sides = cut // BLOCK
     per_tp = count // tp_count
     subs = sides * PARTS
-    pieces = 2 * PIECES + 2 * sides
     anywhere = pl.BlockSpec(memory_space=pl.ANY)
     inside = pl.BlockSpec(memory_space=pltpu.VMEM)
     bf16, f32 = jnp.bfloat16, jnp.float32
@@ -806,10 +846,12 @@
             pltpu.VMEM((length, channels), bf16),
             pltpu.VMEM((channels, width), bf16),
             pltpu.VMEM((half, width), bf16),
-            pltpu.VMEM((length, groups * state_size), bf16),
+            pltpu.VMEM((length // BLOCK, state_size, channels), bf16),
             pltpu.VMEM((length, channels), f32),
             pltpu.VMEM((BLOCK, channels), bf16),
             pltpu.VMEM((state_size, channels), f32),
+            pltpu.VMEM((heads, length), f32),
+            pltpu.VMEM((heads, length), f32),
             pltpu.VMEM((heads, length), f32),
             pltpu.VMEM((heads, BLOCK), f32),
             pltpu.VMEM((inner, state_size + HALO, channels), bf16),
@@ -828,8 +870,8 @@
             pltpu.VMEM((chips - 1, per_tp, subs, length // PARTS, BLOCK), bf16),
             dma((7 + sides,)),
             dma((2, 2)),
-            dma((pieces, 2, hops)),
-            dma((pieces, 2, hops)),
+            dma((2, SLOTS)),
+            dma((2, SLOTS)),
             dma((max(inner - 1, 1),)),
             dma((max(inner - 1, 1),)),
             dma((2, 2)),

time: 195 us -> 190 us (0.974); the launches traced: 191 us -> 190 us
  no operation moved by 1% of the time
where the time goes in v2:
time: 190 us
  Pallas kernels  189 us (99%)
    pallas_call x1, Pallas kernels, shards(): pl.pallas_call(layer_kernel, out_shape=pltpu.VMEM((length, width // tp_co...  189 us

profile of v2, /device:TPU:3, one launch (start us, length us, event | category | flops | bytes accessed | tf_op | source)
XLA Modules:
  0.0 190.0 jit_solution(2800498407921643034)
XLA Ops:
  0.0 189.1 %layer.1 = bf16[1024,512]{1,0:T(8,128)(2,1)S(1)} custom-call(bf16[1024,2048]{1,0:T(8,128)(2,1)} %arriving.1, bf16[1024,1024]{1,0:T(8,128)(2,1)} %content.1, bf16[1024,1024]{1,0:T(8,128)(2,1)} %leaving.1, bf16[4096,128]{1,0:T(8,128)(2,1)} %bitcast.8, bf16[256,1408]{1,0:T(8,128)(2,1)} %gate_own.1, bf16[256,1408]{1,0:T(8,128)(2,1)} %up_own.1, ...), custom_call_target="tpu_custom_call" | custom-call | tf_op jit(solution)/shard_map/layer/pallas_call | solution.py:837
  189.1 1.0 copy.19

commit v3 on v2

--- a/solution.py
+++ b/solution.py
@@ -52,7 +52,7 @@
 
 
 PIECES = 4
-PARTS = 2
+PARTS = 4
 SLOTS = 8
 DEPTH = 3
 
@@ -166,15 +166,22 @@
 
 def layer_kernel(
     arriving, content, leaving, pairs, gate_own, up_own, down_own, blend_hbm,
-    raw, spike, value_taps, map_taps, shift, fading, skip, rescale, gain,
+    raw_hbm, spike_hbm, value_taps_hbm, map_taps_hbm, shift_hbm, fading_hbm, skip_hbm,
+    rescale_hbm, gain_hbm,
     out,
     padded, map_padded, regroup, leave, blend, arrived, entering, mixer, mixed, state,
     cums, steps, reach, prior,
     messages, chain, partial, from_partner, from_across, mid, resid,
     gate, up, hidden, down, made, made_partner, made_across,
     local_sem, halo_sem, ring_send, ring_recv, plane_send, plane_recv, chain_sem,
-    core_sem, across_sem, mid_sem, made_core_sem, made_across_sem,
+    core_sem, across_sem, mid_sem, made_core_send, made_core_recv, made_across_send,
+    made_across_recv, small_sem, *small,
 ):
+    raw, spike, value_taps, map_taps, shift, fading, skip, rescale, gain = small
+    small_hbm = (
+        raw_hbm, spike_hbm, value_taps_hbm, map_taps_hbm, shift_hbm, fading_hbm, skip_hbm,
+        rescale_hbm, gain_hbm,
+    )
     length, channels = content.shape
     heads = raw.shape[0]
     size = channels // heads
@@ -215,8 +222,14 @@
                 down_own.at[:, pl.ds(side * BLOCK, BLOCK)], down.at[me, side], local_sem.at[7 + side]
             )
         )
+    small_loads = [
+        pltpu.make_async_copy(src, dst, small_sem.at[i])
+        for i, (src, dst) in enumerate(zip(small_hbm, small))
+    ]
     loads[0].start()
     loads[1].start()
+    for load in small_loads:
+        load.start()
 
     def rows_piece(own, whole, part):
         tall = depth // PIECES
@@ -296,6 +309,8 @@
     prior[...] = jnp.zeros_like(prior)
     loads[0].wait()
     loads[1].wait()
+    for load in small_loads:
+        load.wait()
 
     @pl.when(me > 0)
     def _():
@@ -679,8 +694,8 @@
         return pltpu.make_async_remote_copy(
             src_ref=made.at[k, unit],
             dst_ref=made_partner.at[slot(k), unit],
-            send_sem=made_core_sem.at[0, k, unit],
-            recv_sem=made_core_sem.at[1, k, unit],
+            send_sem=made_core_send.at[0],
+            recv_sem=made_core_recv.at[slot(k), unit],
             device_id=partner,
             device_id_type=MESH,
         )
@@ -689,8 +704,8 @@
         return pltpu.make_async_remote_copy(
             src_ref=made.at[k, unit],
             dst_ref=made_across.at[into, lax.rem(order[k][0], per_tp), unit],
-            send_sem=made_across_sem.at[0, s, k, unit],
-            recv_sem=made_across_sem.at[1, into, k, unit],
+            send_sem=made_across_send.at[s],
+            recv_sem=made_across_recv.at[into, lax.rem(order[k][0], per_tp), unit],
             device_id=across[s],
             device_id_type=MESH,
         )
@@ -795,20 +810,23 @@
         for s in range(len(across)):
             to_across(s, j).wait_send()
     flow.drain()
-    for k in range(len(order)):
-        goal_chip, goal_core = target(k)
-
-        @pl.when(goal_core != core)
-        def _():
-            for unit in range(len(units_of)):
-                over_cores(k, unit).wait_send()
-
-        for s in range(chips - 1):
-
-            @pl.when((goal_core == core) & (goal_chip == lax.rem(chip + s + 1, chips)))
-            def _():
-                for unit in range(len(units_of)):
-                    over_chips(k, unit, s, chips - 2 - s).wait_send()
+    pltpu.make_async_remote_copy(
+        src_ref=made.at[: chips * per_tp],
+        dst_ref=made_partner,
+        send_sem=made_core_send.at[0],
+        recv_sem=made_core_recv.at[0, 0],
+        device_id=partner,
+        device_id_type=MESH,
+    ).wait_send()
+    for s in range(chips - 1):
+        pltpu.make_async_remote_copy(
+            src_ref=made.at[:per_tp],
+            dst_ref=made_across.at[s],
+            send_sem=made_across_send.at[s],
+            recv_sem=made_across_recv.at[s, 0, 0],
+            device_id=across[s],
+            device_id_type=MESH,
+        ).wait_send()
 
 
 def shards(
@@ -834,10 +852,14 @@
     inside = pl.BlockSpec(memory_space=pltpu.VMEM)
     bf16, f32 = jnp.bfloat16, jnp.float32
     dma = pltpu.SemaphoreType.DMA
+    small = (
+        raw.T, spike.T, value_taps, map_taps,
+        shift[None], fading[None], skip[None], rescale[None], gain[None],
+    )
     return pl.pallas_call(
         layer_kernel,
         out_shape=pltpu.VMEM((length, width // tp_count), bf16),
-        in_specs=[anywhere] * 8 + [inside] * 9,
+        in_specs=[anywhere] * (8 + len(small)),
         out_specs=inside,
         scratch_shapes=[
             pltpu.VMEM((HALO + length, channels), bf16),
@@ -878,8 +900,12 @@
             dma((2, half_blocks)),
             dma((2, chips - 1, half_blocks)),
             dma((2, half_blocks)),
-            dma((2, count, subs)),
-            dma((2, chips - 1, count, subs)),
+            dma((1,)),
+            dma((chips * per_tp, subs)),
+            dma((chips - 1,)),
+            dma((chips - 1, per_tp, subs)),
+            dma((len(small),)),
+            *[pltpu.VMEM(x.shape, x.dtype) for x in small],
         ],
         compiler_params=pltpu.CompilerParams(
             collective_id=0, has_side_effects=True, vmem_limit_bytes=VMEM_BYTES
@@ -887,8 +913,7 @@
         name="layer",
     )(
         arriving, content, leaving, linked.reshape(length * kinds, state_size), gate, up, down, blend,
-        raw.T, spike.T, value_taps, map_taps,
-        shift[None], fading[None], skip[None], rescale[None], gain[None],
+        *small,
     )
 
 

time: 190 us -> 188 us (0.989)
  Pallas kernels: 189 us -> 187 us
    pallas_call x1, Pallas kernels: 189 us -> 187 us  [shards(): pl.pallas_call(layer_kernel, out_shape=pltpu.VMEM((length, width // tp_co...]
where the time goes in v3:
time: 188 us
  Pallas kernels  187 us (99%)
    pallas_call x1, Pallas kernels, shards(): pl.pallas_call(layer_kernel, out_shape=pltpu.VMEM((length, width // tp_co...  187 us

profile of v3, /device:TPU:3, one launch (start us, length us, event | category | flops | bytes accessed | tf_op | source)
XLA Modules:
  0.0 187.7 jit_solution(12654051988324249308)
XLA Ops:
  0.0 186.7 %layer.1 = bf16[1024,512]{1,0:T(8,128)(2,1)S(1)} custom-call(bf16[1024,2048]{1,0:T(8,128)(2,1)} %arriving.1, bf16[1024,1024]{1,0:T(8,128)(2,1)} %content.1, bf16[1024,1024]{1,0:T(8,128)(2,1)} %leaving.1, bf16[4096,128]{1,0:T(8,128)(2,1)} %bitcast.8, bf16[256,1408]{1,0:T(8,128)(2,1)} %gate_own.1, bf16[256,1408]{1,0:T(8,128)(2,1)} %up_own.1, ...), custom_call_target="tpu_custom_call" | custom-call | tf_op jit(solution)/shard_map/layer/pallas_call | solution.py:859
  186.7 1.0 copy.19

commit v4 on v3

--- a/solution.py
+++ b/solution.py
@@ -58,11 +58,12 @@
 
 
 class Flow:
-    def __init__(self, sets, send_sem, recv_sem):
+    def __init__(self, sets, send_sem, recv_sem, pair_sem, partner):
         count = lax.axis_size("sp")
         spot = ring_spot(lax.axis_index("sp"), count)
         self.count, self.hops, self.spot = count, count // 2, spot
         self.send_sem, self.recv_sem = send_sem, recv_sem
+        self.pair_sem, self.partner = pair_sem, partner
         self.pieces = [piece for group in sets for piece in group]
         self.next = (
             ring_at(lax.rem(spot + 1, count), count),
@@ -118,6 +119,10 @@
     def step(self, times=1):
         for _ in range(times):
             self.pull()
+            pl.semaphore_signal(
+                self.pair_sem, inc=1, device_id=self.partner, device_id_type=MESH
+            )
+            pl.semaphore_wait(self.pair_sem, 1)
             self.push()
 
     def until(self, pulled):
@@ -175,7 +180,7 @@
     gate, up, hidden, down, made, made_partner, made_across,
     local_sem, halo_sem, ring_send, ring_recv, plane_send, plane_recv, chain_sem,
     core_sem, across_sem, mid_sem, made_core_send, made_core_recv, made_across_send,
-    made_across_recv, small_sem, *small,
+    made_across_recv, pair_sem, small_sem, *small,
 ):
     raw, spike, value_taps, map_taps, shift, fading, skip, rescale, gain = small
     small_hbm = (
@@ -259,6 +264,8 @@
         ],
         ring_send,
         ring_recv,
+        pair_sem,
+        partner,
     )
     fed = flow.ends[flow.hops - 1]
     before = {"sp": lax.rem(me + count - 1, count)}
@@ -445,7 +452,7 @@
 
     def local_step(turn, _):
         lax.fori_loop(2 * turn, 2 * turn + 2, state_step, 0)
-        flow.paced(turn, [0, 0, 0, 1])
+        flow.paced(turn, [0, 0, 1, 1])
         return 0
 
     lax.fori_loop(0, blocks // 2, local_step, 0)
@@ -904,6 +911,7 @@
             dma((chips * per_tp, subs)),
             dma((chips - 1,)),
             dma((chips - 1, per_tp, subs)),
+            pltpu.SemaphoreType.REGULAR,
             dma((len(small),)),
             *[pltpu.VMEM(x.shape, x.dtype) for x in small],
         ],

time: 188 us -> 185 us (0.984)
  Pallas kernels: 187 us -> 184 us
    pallas_call x1, Pallas kernels: 187 us -> 184 us  [shards(): pl.pallas_call(layer_kernel, out_shape=pltpu.VMEM((length, width // tp_co...]
where the time goes in v4:
time: 185 us
  Pallas kernels  184 us (99%)
    pallas_call x1, Pallas kernels, shards(): pl.pallas_call(layer_kernel, out_shape=pltpu.VMEM((length, width // tp_co...  184 us

profile of v4, /device:TPU:3, one launch (start us, length us, event | category | flops | bytes accessed | tf_op | source)
XLA Modules:
  0.0 185.1 jit_solution(2279216838278650069)
XLA Ops:
  0.0 184.1 %layer.1 = bf16[1024,512]{1,0:T(8,128)(2,1)S(1)} custom-call(bf16[1024,2048]{1,0:T(8,128)(2,1)} %arriving.1, bf16[1024,1024]{1,0:T(8,128)(2,1)} %content.1, bf16[1024,1024]{1,0:T(8,128)(2,1)} %leaving.1, bf16[4096,128]{1,0:T(8,128)(2,1)} %bitcast.8, bf16[256,1408]{1,0:T(8,128)(2,1)} %gate_own.1, bf16[256,1408]{1,0:T(8,128)(2,1)} %up_own.1, ...), custom_call_target="tpu_custom_call" | custom-call | tf_op jit(solution)/shard_map/layer/pallas_call | solution.py:866
  184.1 1.0 copy.19
